TPU v7x, 32 devices: a whole 2x2x4 slice. The times are simulated.
32 devices in a mesh: rep: 2 (over y), fs: 4 (over z), tp: 4 (over x, core).
Axes of the slice: x: 2, y: 2, z: 4, core: 2. Of those that a mesh axis runs over, the one named last changes fastest.
Arguments:
- tokens: bfloat16 [4096, 2048], P(('rep', 'fs')), may hold values from -6 to 6
- norm_gain: float32 [2048], replicated, may hold values from 0.1 to 1.9
- gate_weight: bfloat16 [2048, 5632], P('fs', 'tp'), may hold values from -0.125 to 0.125
- up_weight: bfloat16 [2048, 5632], P('fs', 'tp'), may hold values from -0.125 to 0.125
- down_weight: bfloat16 [5632, 2048], P('tp', 'fs'), may hold values from -0.078125 to 0.078125
Outputs:
- branch_out: bfloat16 [4096, 2048], P(('rep', 'fs'))
All inputs are finite; a program needn't handle non-finite values.
Results may differ from a plain program's by a relative error of at most 0.014.
Values may be sent and summed in bfloat16 or wider, within the bound.
A program may use at most 64 MiB of HBM per device.

v0:
```python
import jax
import jax.numpy as jnp
from jax import lax
from jax.sharding import PartitionSpec as P


def add_rows(left, piece):
    return jnp.dot(left, piece, preferred_element_type=jnp.float32)


def per_device(tokens, norm_gain, gate_weight, up_weight, down_weight):
    wide_tok = tokens.astype(jnp.float32)
    scale = lax.rsqrt(jnp.mean(wide_tok * wide_tok, axis=-1, keepdims=True) + 1e-06)
    normed = (wide_tok * scale * norm_gain).astype(jnp.bfloat16)

    def add_one(piece):
        return add_rows(normed, piece)

    gate = add_one(lax.all_gather(gate_weight, "fs", axis=0, tiled=True))
    up = add_one(lax.all_gather(up_weight, "fs", axis=0, tiled=True))
    hidden = (jax.nn.silu(gate) * up).astype(jnp.bfloat16)
    partial_value = jnp.dot(
        hidden,
        lax.all_gather(down_weight, "fs", axis=1, tiled=True),
        preferred_element_type=jnp.float32,
    )
    return lax.psum(partial_value.astype(jnp.bfloat16), "tp")


def solution(mesh):
    in_specs = (P(("rep", "fs"), None), P(), P("fs", "tp"), P("fs", "tp"), P("tp", "fs"))
    out_specs = P(("rep", "fs"), None)
    return jax.shard_map(
        per_device, mesh=mesh, in_specs=in_specs, out_specs=out_specs, check_vma=False
    )
```

profile of v0, /device:TPU:0, one launch (start us, length us, event | category | flops | bytes accessed | tf_op | source)
XLA Modules:
  0.0 404.2 jit_solution(18413360618791287892)
XLA Ops:
  6.5 0.0 copy-start
  6.5 0.0 copy-start.1
  6.5 0.0 all-gather.4.cloned.1.call-start
  6.5 0.7 all-gather.4.cloned.1.call-update
  7.3 0.0 all-gather.6.cloned.1.call-start
  7.3 0.7 all-gather.6.cloned.1.call-update
  8.0 0.0 all-gather.8.cloned.1.call-start
  8.1 0.7 all-gather.8.cloned.1.call-update
  8.7 0.0 all-reduce.2.cloned.1.call-start
  8.8 0.0 copy-done
  8.8 0.5 fusion
  9.3 109.1 %all-gather.4.cloned.1.call-done = bf16[2048,1408]{1,0:T(8,128)(2,1)} async-done(((bf16[512,1408]{1,0:T(8,128)(2,1)}), bf16[2048,1408]{1,0:T(8,128)(2,1)}) %all-gather.4.cloned.1.call-update) | async-done | bytes 5767184 | tf_op jit(solution)/shard_map/all_gather | solution.py:19
  118.3 0.0 copy-done.1
  118.4 7.6 %fusion.6 = f32[512,1408]{1,0:T(8,128)} fusion(bf16[2048,1408]{1,0:T(8,128)(2,1)} %all-gather.4.cloned.1.call-done, bf16[512,2048]{1,0:T(8,128)(2,1)S(1)} %copy-done, f32[2048]{0:T(1024)S(1)} %copy-done.1, f32[512]{0:T(512)S(1)} %add_rsqrt_fusion), kind=kOutput, calls=%fused_computation.8 | convolution fusion | flops 2956984320 | bytes 10758144 | tf_op jit(solution)/shard_map/dot_general | solution.py:8
  126.0 98.9 %all-gather.6.cloned.1.call-done = bf16[2048,1408]{1,0:T(8,128)(2,1)} async-done(((bf16[512,1408]{1,0:T(8,128)(2,1)}), bf16[2048,1408]{1,0:T(8,128)(2,1)}) %all-gather.6.cloned.1.call-update) | async-done | bytes 5767184 | tf_op jit(solution)/shard_map/all_gather | solution.py:20
  224.9 106.5 %all-gather.8.cloned.1.call-done = bf16[1408,2048]{1,0:T(8,128)(2,1)} async-done(((bf16[1408,512]{1,0:T(8,128)(2,1)}), bf16[1408,2048]{1,0:T(8,128)(2,1)}) %all-gather.8.cloned.1.call-update) | async-done | bytes 5767184 | tf_op jit(solution)/shard_map/all_gather | solution.py:24
  331.4 13.3 %convolution_convert_fusion = bf16[512,2048]{1,0:T(8,128)(2,1)} fusion(bf16[1408,2048]{1,0:T(8,128)(2,1)} %all-gather.8.cloned.1.call-done, bf16[2048,1408]{1,0:T(8,128)(2,1)} %all-gather.6.cloned.1.call-done, f32[512,1408]{1,0:T(8,128)} %fusion.6, bf16[512,2048]{1,0:T(8,128)(2,1)S(1)} %copy-done, f32[2048]{0:T(1024)S(1)} %copy-done.1, f32[512]{0:T(512)S(1)} %add_rsqrt_fusion), kind=kOutput, calls=%fused_computation.7 | convolution fusion | flops 5915148288 | bytes 18622464 | tf_op jit(solution)/shard_map/dot_general | solution.py:22
  344.7 0.0 all-reduce.2.cloned.1.call-update
  344.7 49.8 %all-reduce.2.cloned.1.call-done = bf16[512,2048]{1,0:T(8,128)(2,1)} async-done(((bf16[512,2048]{1,0:T(8,128)(2,1)}), bf16[512,2048]{1,0:T(8,128)(2,1)}) %all-reduce.2.cloned.1.call-update) | async-done | bytes 2097168 | tf_op jit(solution)/shard_map/psum | solution.py:27
  394.5 3.2 copy.7
  (1 shorter events, 0.0 us)
Async XLA Ops:
  6.5 2.3 copy-start
  6.5 111.8 %copy-start.1 = (f32[2048]{0:T(1024)S(1)}, f32[2048]{0:T(1024)}, u32[]{:S(2)}) copy-start(f32[2048]{0:T(1024)} %param.6) | copy-start | bytes 24580
  6.5 111.8 %all-gather.4.cloned.1.call-start = ((), (), s32[]{:S(2)}) async-start(), calls=%async_computation | async-start | bytes 7208960 | tf_op jit(solution)/shard_map/all_gather | solution.py:19
  7.3 217.6 %all-gather.6.cloned.1.call-start = ((), (), s32[]{:S(2)}) async-start(), calls=%async_computation.1 | async-start | bytes 7208960 | tf_op jit(solution)/shard_map/all_gather | solution.py:20
  8.0 323.4 %all-gather.8.cloned.1.call-start = ((), (), s32[]{:S(2)}) async-start(), calls=%async_computation.2 | async-start | bytes 7208960 | tf_op jit(solution)/shard_map/all_gather | solution.py:24
  8.7 385.8 %all-reduce.2.cloned.1.call-start = ((), (), s32[]{:S(2)}) async-start(), calls=%async_computation.3 | async-start | bytes 4194304 | tf_op jit(solution)/shard_map/psum | solution.py:27
Sparse Core Ops, SparseCore 0:
  8.9 109.3 all-gather.3
  119.9 104.9 all-gather.5
  226.5 104.9 all-gather.7
  344.9 49.6 all-reduce.1
where the time goes:
time: 404 us
  waiting for transfers between devices  366 us (91%)
  matrix products  20.9 us (5%)
  between operations  13.1 us (3%)
    all_gather x1, waiting for transfers between devices, per_device(): gate = add_one(lax.all_gather(gate_weight, 'fs', axis=0, tiled=True))  109 us
    all_gather x1, waiting for transfers between devices, per_device(): lax.all_gather(down_weight, 'fs', axis=1, tiled=True)  107 us
    all_gather x1, waiting for transfers between devices, per_device(): up = add_one(lax.all_gather(up_weight, 'fs', axis=0, tiled=True))  98.9 us
    psum x1, waiting for transfers between devices, per_device(): return lax.psum(partial_value.astype(jnp.bfloat16), 'tp')  49.8 us
    dot_general x1, matrix products, per_device(): jnp.dot(hidden, lax.all_gather(down_weight, 'fs', axis=1, tiled=True), pr...  13.3 us
  transfers between devices with their start and end apart: 4, of which 4 were waited for; matrix products, arithmetic and copies ran while one was open for 2% of the time, Pallas kernels for 0%

commit v1 on v0

v1 whole, which is shorter than its diff:
```python
import functools

import jax
import jax.numpy as jnp
from jax import lax
from jax.experimental import pallas as pl
from jax.experimental.pallas import tpu as pltpu
from jax.sharding import PartitionSpec as P

MESH = pl.DeviceIdType.MESH
F32 = jnp.float32
BF16 = jnp.bfloat16


def plain(tokens, norm_gain, gate_weight, up_weight, down_weight):
    wide_tok = tokens.astype(F32)
    scale = lax.rsqrt(jnp.mean(wide_tok * wide_tok, axis=-1, keepdims=True) + 1e-06)
    normed = (wide_tok * scale * norm_gain).astype(BF16)
    gate = jnp.dot(normed, lax.all_gather(gate_weight, "fs", axis=0, tiled=True), preferred_element_type=F32)
    up = jnp.dot(normed, lax.all_gather(up_weight, "fs", axis=0, tiled=True), preferred_element_type=F32)
    hidden = (jax.nn.silu(gate) * up).astype(BF16)
    down = lax.all_gather(down_weight, "fs", axis=1, tiled=True)
    partial_value = jnp.dot(hidden, down, preferred_element_type=F32)
    return lax.psum(partial_value.astype(BF16), "tp")


CHUNKS = 2
LAG = 2


def kernel(
    n, tok_ref, gain_ref, wg_ref, wu_ref, wd_ref, out_ref,
    normed, bg, bu, bd, gate, up, hidden, part, r1, sbuf, r2, outv,
    loc_sem, zsend, zrecv, ysend, yrecv, psend, precv, xsend, xrecv, qsend, qrecv, osem,
):
    z = lax.axis_index("fs")
    y = lax.axis_index("rep")
    t = lax.axis_index("tp")
    c = lax.rem(t, 2)
    tokens, width = tok_ref.shape
    depth, units = wg_ref.shape
    cols = wd_ref.shape[1] // CHUNKS
    half_k, half_u, half_t = depth // 2, units // 2, tokens // 2
    mate = {"tp": t + 1 - 2 * c}
    across = {"tp": lax.rem(t + 2, 4)}
    peer = {"rep": 1 - y}

    barrier = pltpu.get_barrier_semaphore()

    around = ({"fs": lax.rem(z + 1, n)}, {"fs": lax.rem(z + n - 1, n)})
    for one in around + (mate, across, peer):
        pl.semaphore_signal(barrier, 1, device_id=one, device_id_type=MESH)
    pl.semaphore_wait(barrier, 5)

    def rows_of(u, who):
        size = half_k if u < 2 else half_u
        return pl.ds(pl.multiple_of(who * size, size), size)

    def slot(u, blk, who):
        if u == 0:
            return bg.at[blk, rows_of(u, who)]
        if u == 1:
            return bu.at[blk, rows_of(u, who)]
        return bd.at[blk, u - 2, rows_of(u, who)]

    def own(u):
        if u == 0:
            return wg_ref.at[rows_of(u, y)]
        if u == 1:
            return wu_ref.at[rows_of(u, y)]
        return wd_ref.at[rows_of(u, y), pl.ds((u - 2) * cols, cols)]

    def along(u, blk, way, src=None):
        return pltpu.make_async_remote_copy(
            src_ref=slot(u, blk, y) if src is None else src,
            dst_ref=slot(u, blk, y),
            send_sem=zsend.at[u, blk, way],
            recv_sem=zrecv.at[u, blk],
            device_id={"fs": z - 1 + 2 * way},
            device_id_type=MESH,
        )

    def swap(u, blk, who):
        return pltpu.make_async_remote_copy(
            src_ref=slot(u, blk, who),
            dst_ref=slot(u, blk, who),
            send_sem=ysend.at[u, blk],
            recv_sem=yrecv.at[u, blk],
            device_id=peer,
            device_id_type=MESH,
        )

    def send_own(units_now, way):
        for u in units_now:
            along(u, z, way, own(u)).start()

    D_UNITS = tuple(range(2, 2 + CHUNKS))
    pl.when(z > 0)(lambda: send_own((0, 1), 0))
    pl.when(z < n - 1)(lambda: send_own((0, 1), 1))
    pl.when(z == n - 1)(lambda: send_own(D_UNITS, 0))
    pl.when(z == 0)(lambda: send_own(D_UNITS, 1))

    locals_ = [
        pltpu.make_async_copy(wg_ref, bg.at[z], loc_sem.at[0]),
        pltpu.make_async_copy(wu_ref, bu.at[z], loc_sem.at[1]),
    ] + [
        pltpu.make_async_copy(wd_ref.at[:, pl.ds(j * cols, cols)], bd.at[z, j], loc_sem.at[2 + j])
        for j in range(CHUNKS)
    ]
    for copy in locals_:
        copy.start()

    step = 64

    @pl.loop(0, tokens // step)
    def _(i):
        at = pl.ds(pl.multiple_of(i * step, step), step)
        wide = tok_ref[at, :].astype(F32)
        scale = lax.rsqrt(jnp.mean(wide * wide, axis=-1, keepdims=True) + 1e-06)
        normed[at, :] = (wide * scale * gain_ref[...]).astype(BF16)

    def add_dot(u, blk, first=False):
        total, held = (gate, bg) if u == 0 else (up, bu)

        @pl.loop(0, 2)
        def _(i):
            at = pl.ds(pl.multiple_of(i * half_t, half_t), half_t)
            left = normed[at, pl.ds(pl.multiple_of(blk * depth, depth), depth)]
            value = jnp.dot(left, held[blk], preferred_element_type=F32)
            total[at, :] = value if first else total[at, :] + value

    def place(blk, j, who):
        return (
            pl.ds(pl.multiple_of(who * half_t, half_t), half_t),
            pl.ds(pl.multiple_of(blk * (cols * CHUNKS) + j * cols, cols), cols),
        )

    def to_mate(blk, j):
        return pltpu.make_async_remote_copy(
            part.at[blk, j, 1], r1.at[blk, j], psend.at[blk, j], precv.at[blk, j],
            device_id=mate, device_id_type=MESH)

    def to_across(blk, j):
        return pltpu.make_async_remote_copy(
            sbuf.at[blk, j], r2.at[blk, j], xsend.at[blk, j], xrecv.at[blk, j],
            device_id=across, device_id_type=MESH)

    def give(blk, j, who):
        return pltpu.make_async_remote_copy(
            outv.at[place(blk, j, who)], outv.at[place(blk, j, who)], qsend.at[blk, j], qrecv.at[blk, j],
            device_id=mate, device_id_type=MESH)

    def write(blk, j):
        at = pl.ds(pl.multiple_of(blk * (cols * CHUNKS) + j * cols, cols), cols)
        return pltpu.make_async_copy(outv.at[:, at], out_ref.at[:, at], osem.at[blk, j])

    def make_part(blk, j):
        @pl.loop(0, 2)
        def _(i):
            side = 1 - i
            whose = c + side - 2 * c * side
            at = pl.ds(pl.multiple_of(whose * half_t, half_t), half_t)
            value = jnp.dot(hidden[at, :], bd[blk, j], preferred_element_type=F32)
            part[blk, j, side] = value.astype(BF16)

        to_mate(blk, j).start()

    def add_pair(blk, j):
        to_mate(blk, j).wait_recv()
        sbuf[blk, j] = (part[blk, j, 0].astype(F32) + r1[blk, j].astype(F32)).astype(BF16)
        to_across(blk, j).start()

    def finish(blk, j):
        to_across(blk, j).wait_recv()
        outv[place(blk, j, c)] = (sbuf[blk, j].astype(F32) + r2[blk, j].astype(F32)).astype(BF16)
        give(blk, j, c).start()

    def store(blk, j):
        give(blk, j, 1 - c).wait_recv()
        write(blk, j).start()

    def sides(k, body):
        @pl.loop(0, 2)
        def _(way):
            blk = z + k - 2 * k * way

            @pl.when(jnp.logical_and(blk >= 0, blk < n))
            def _():
                body(blk, way)

    def forward(u, k):
        def body(blk, way):
            along(u, blk, way).wait_recv()

            @pl.when(jnp.logical_or(jnp.logical_and(way == 0, z > 0), jnp.logical_and(way == 1, z < n - 1)))
            def _():
                along(u, blk, way).start()

            swap(u, blk, y).start()

        sides(k, body)

    def both(body, blk, j):
        body(blk, j)

    behind = []

    def use(u, k):
        if u < 2:
            def body(blk, way):
                swap(u, blk, 1 - y).wait_recv()
                add_dot(u, blk)

            sides(k, body)
            return

        def body(blk, way):
            swap(u, blk, 1 - y).wait_recv()
            make_part(blk, u - 2)

        sides(k, body)
        advance(k, u - 2)

    def advance(k, j):
        if behind:
            old = behind.pop()
            run(old[0], lambda blk: finish(blk, old[1]))
            late.append(old)
        run(k, lambda blk: add_pair(blk, j))
        if late:
            old = late.pop()
            run(old[0], lambda blk: store(blk, old[1]))
        behind.append((k, j))

    late = []

    def run(k, body):
        if k == 0:
            body(z)
        else:
            sides(k, lambda blk, way: body(blk))

    def middle():
        @pl.loop(0, tokens // step)
        def _(i):
            at = pl.ds(pl.multiple_of(i * step, step), step)
            value = gate[at, :]
            hidden[at, :] = (value / (1.0 + jnp.exp(-value)) * up[at, :]).astype(BF16)

        for j in range(CHUNKS):
            locals_[2 + j].wait()
            make_part(z, j)
            advance(0, j)

    for u in (0, 1):
        locals_[u].wait()
        add_dot(u, z, first=True)

    events = [(u, k) for k in range(1, n) for u in (0, 1)]
    last_row = len(events)
    events += [(u, k) for k in range(1, n) for u in D_UNITS]
    for i in range(len(events) + LAG):
        if i < len(events):
            u, k = events[i]
            forward(u, k)
            if u == 1:
                pl.when(jnp.logical_and(n - 1 - z == k, z > 0))(lambda: send_own(D_UNITS, 0))
                pl.when(jnp.logical_and(z == k, z < n - 1))(lambda: send_own(D_UNITS, 1))
        if i >= LAG:
            use(*events[i - LAG])
            if i - LAG == last_row - 1:
                middle()
    k, j = behind.pop()
    run(k, lambda blk: finish(blk, j))
    run(k, lambda blk: store(blk, j))

    for u in range(2 + CHUNKS):
        pl.when(z > 0)(lambda: along(u, z, 0, own(u)).wait_send())
        pl.when(z < n - 1)(lambda: along(u, z, 1, own(u)).wait_send())
        for k in range(1, n):
            def sent(blk, way):
                @pl.when(jnp.logical_or(jnp.logical_and(way == 0, z > 0), jnp.logical_and(way == 1, z < n - 1)))
                def _():
                    along(u, blk, way).wait_send()

                swap(u, blk, y).wait_send()

            sides(k, sent)

    @pl.loop(0, n)
    def _(blk):
        for j in range(CHUNKS):
            to_mate(blk, j).wait_send()
            to_across(blk, j).wait_send()
            give(blk, j, c).wait_send()
            write(blk, j).wait()


def fused(n, tokens, norm_gain, gate_weight, up_weight, down_weight):
    rows, width = tokens.shape
    depth, units = gate_weight.shape
    cols = down_weight.shape[1] // CHUNKS
    dma = pltpu.SemaphoreType.DMA
    grid_of = (n, CHUNKS)
    hbm = pl.BlockSpec(memory_space=pl.ANY)
    vmem = pl.BlockSpec(memory_space=pltpu.VMEM)
    return pl.pallas_call(
        functools.partial(kernel, n),
        out_shape=jax.ShapeDtypeStruct((rows, width), BF16),
        in_specs=[vmem, vmem, hbm, hbm, hbm],
        out_specs=hbm,
        scratch_shapes=[
            pltpu.VMEM((rows, width), BF16),
            pltpu.VMEM((n, depth, units), BF16),
            pltpu.VMEM((n, depth, units), BF16),
            pltpu.VMEM((n, CHUNKS, units, cols), BF16),
            pltpu.VMEM((rows, units), F32),
            pltpu.VMEM((rows, units), F32),
            pltpu.VMEM((rows, units), BF16),
            pltpu.VMEM((n, CHUNKS, 2, rows // 2, cols), BF16),
            pltpu.VMEM((n, CHUNKS, rows // 2, cols), BF16),
            pltpu.VMEM((n, CHUNKS, rows // 2, cols), BF16),
            pltpu.VMEM((n, CHUNKS, rows // 2, cols), BF16),
            pltpu.VMEM((rows, width), BF16),
            dma((2 + CHUNKS,)),
            dma((2 + CHUNKS, n, 2)),
            dma((2 + CHUNKS, n)),
            dma((2 + CHUNKS, n)),
            dma((2 + CHUNKS, n)),
        ] + [dma(grid_of) for _ in range(7)],
        compiler_params=pltpu.CompilerParams(
            collective_id=0, has_side_effects=True, vmem_limit_bytes=60 * 2**20
        ),
    )(tokens, norm_gain.reshape(1, width), gate_weight, up_weight, down_weight)


def solution(mesh):
    n = mesh.shape["fs"]
    small = mesh.shape["rep"] == 2 and mesh.shape["tp"] == 4 and n <= 4
    body = functools.partial(fused, n) if small else plain
    in_specs = (P(("rep", "fs"), None), P(), P("fs", "tp"), P("fs", "tp"), P("tp", "fs"))
    out_specs = P(("rep", "fs"), None)
    return jax.shard_map(
        body, mesh=mesh, in_specs=in_specs, out_specs=out_specs, check_vma=False
    )
```

time: 404 us -> 175 us (0.43)
  waiting for transfers between devices: 366 us -> 0 us
  Pallas kernels: 0 us -> 172 us
  matrix products: 20.9 us -> 0 us
  between operations: 13.1 us -> 0.01 us
    all_gather x3 -> x0, waiting for transfers between devices: 315 us -> none  [the longest x1 109 us: per_device(): gate = add_one(lax.all_gather(gate_weight, 'fs', axis=0, tiled=True))]
    pallas_call x0 -> x1, Pallas kernels: none -> 172 us  [fused(): pl.pallas_call(functools.partial(kernel, n), out_shape=jax.ShapeDtypeStru...]
    psum x1 -> x0, waiting for transfers between devices: 49.8 us -> none  [per_device(): return lax.psum(partial_value.astype(jnp.bfloat16), 'tp')]
    dot_general x2 -> x0, matrix products: 20.9 us -> none  [the longest x1 13.3 us: per_device(): jnp.dot(hidden, lax.all_gather(down_weight, 'fs', axis=1, tiled=True), pr...]
  transfers between devices with their start and end apart: 4 -> 0, of which waited for: 4 -> 0; matrix products, arithmetic and copies ran while one was open for 2% -> 0% of each run, Pallas kernels for 0% -> 0%
where the time goes in v1:
time: 175 us
  Pallas kernels  172 us (98%)
  local copies, waits for them, and re-layouts  3.16 us (2%)
    pallas_call x1, Pallas kernels, fused(): pl.pallas_call(functools.partial(kernel, n), out_shape=jax.ShapeDtypeStru...  172 us

profile of v1, /device:TPU:0, one launch (start us, length us, event | category | flops | bytes accessed | tf_op | source)
XLA Modules:
  0.0 175.2 jit_solution(8231383801991355859)
XLA Ops:
  0.0 172.0 %shard_map.55 = bf16[512,2048]{1,0:T(8,128)(2,1)} custom-call(bf16[512,2048]{1,0:T(8,128)(2,1)} %tok_ref.1, f32[1,2048]{1,0:T(1,128)} %bitcast.1, bf16[512,1408]{1,0:T(8,128)(2,1)} %wg_ref.1, bf16[512,1408]{1,0:T(8,128)(2,1)} %wu_ref.1, bf16[1408,512]{1,0:T(8,128)(2,1)} %wd_ref.1), custom_call_target="tpu_custom_call" | custom-call | tf_op jit(solution)/shard_map/pallas_call | solution.py:307
  172.1 3.2 %copy.7 = bf16[512,2048]{1,0:T(8,128)(2,1)} copy(bf16[512,2048]{1,0:T(8,128)(2,1)} %shard_map.55) | data formatting | bytes 4194304

commit v2 on v1

v2 whole, which is shorter than its diff:
```python
import functools

import jax
import jax.numpy as jnp
from jax import lax
from jax.experimental import pallas as pl
from jax.experimental.pallas import tpu as pltpu
from jax.sharding import PartitionSpec as P

MESH = pl.DeviceIdType.MESH
F32 = jnp.float32
BF16 = jnp.bfloat16


def plain(tokens, norm_gain, gate_weight, up_weight, down_weight):
    wide_tok = tokens.astype(F32)
    scale = lax.rsqrt(jnp.mean(wide_tok * wide_tok, axis=-1, keepdims=True) + 1e-06)
    normed = (wide_tok * scale * norm_gain).astype(BF16)
    gate = jnp.dot(normed, lax.all_gather(gate_weight, "fs", axis=0, tiled=True), preferred_element_type=F32)
    up = jnp.dot(normed, lax.all_gather(up_weight, "fs", axis=0, tiled=True), preferred_element_type=F32)
    hidden = (jax.nn.silu(gate) * up).astype(BF16)
    down = lax.all_gather(down_weight, "fs", axis=1, tiled=True)
    partial_value = jnp.dot(hidden, down, preferred_element_type=F32)
    return lax.psum(partial_value.astype(BF16), "tp")


CHUNKS = 2
LAG = 2


def kernel(
    n, tok_ref, gain_ref, wg_ref, wu_ref, wd_ref, out_ref,
    tokp, normed, bg, bu, bd, gate, up, hidden, part, r1, sbuf, rz, sx, r2, outv,
    loc_sem, zsend, zrecv, ysend, yrecv, tsend, trecv,
    psend, precv, wsend, wrecv, xsend, xrecv, qsend, qrecv, osem,
):
    z = lax.axis_index("fs")
    y = lax.axis_index("rep")
    t = lax.axis_index("tp")
    c = lax.rem(t, 2)
    tokens, width = tok_ref.shape
    depth, units = wg_ref.shape
    cols = wd_ref.shape[1] // CHUNKS
    half_k, half_t, quarter = depth // 2, tokens // 2, tokens // 4
    mid = 128
    most = (units - mid) // 2
    e = lax.rem(z, 2)
    low = z - e
    pair = {"fs": z + 1 - 2 * e}
    has_mid = e == c
    parts = ((0, most, 0), (most, mid, c), (most + mid, most, 1))
    mine = pl.multiple_of(e * (most + mid), mid)
    spans = ((mine, most), (most, mid))
    mate = {"tp": t + 1 - 2 * c}
    across = {"tp": lax.rem(t + 2, 4)}
    peer = {"rep": 1 - y}

    barrier = pltpu.get_barrier_semaphore()

    around = ({"fs": lax.rem(z + 1, n)}, {"fs": lax.rem(z + n - 1, n)})
    others = tuple({"tp": lax.rem(t + d, 4)} for d in (1, 2, 3))
    for one in around + others + (peer,):
        pl.semaphore_signal(barrier, 1, device_id=one, device_id_type=MESH)
    pl.semaphore_wait(barrier, 6)

    def token_move(quart, to, sem, first):
        at = pl.ds(pl.multiple_of(quart * quarter, quarter), quarter)
        return pltpu.make_async_remote_copy(
            src_ref=(tok_ref if first else tokp).at[at],
            dst_ref=tokp.at[at],
            send_sem=tsend.at[sem],
            recv_sem=trecv.at[quart],
            device_id=to,
            device_id_type=MESH,
        )

    token_move(t, pair, 0, True).start()

    def window(u, span, who):
        start, size = span
        if u < 2:
            return (pl.ds(pl.multiple_of(who * half_k, half_k), half_k), pl.ds(start, size))
        row = start + who * (size // 2)
        return (pl.ds(pl.multiple_of(row, 64), size // 2),)

    def slot(u, blk, span, who):
        if u < 2:
            return (bg, bu)[u].at[(blk,) + window(u, span, who)]
        return bd.at[(blk, u - 2) + window(u, span, who)]

    def own(u, span):
        if u < 2:
            return (wg_ref, wu_ref)[u].at[window(u, span, y)]
        return wd_ref.at[window(u, span, y) + (pl.ds((u - 2) * cols, cols),)]

    def along(u, blk, p, way, first=False):
        span = parts[p][:2]
        return pltpu.make_async_remote_copy(
            src_ref=own(u, span) if first else slot(u, blk, span, y),
            dst_ref=slot(u, blk, span, y),
            send_sem=zsend.at[u, blk, p, way],
            recv_sem=zrecv.at[u, blk, p],
            device_id={"fs": z - 1 + 2 * way},
            device_id_type=MESH,
        )

    def passes(p, way):
        q = parts[p][2]
        return jnp.logical_or(
            jnp.logical_and(way == 0, z > q), jnp.logical_and(way == 1, z < n - 2 + q))

    def arrives(p, way):
        q = parts[p][2]
        return jnp.logical_or(
            jnp.logical_and(way == 0, z >= q), jnp.logical_and(way == 1, z < n - 1 + q))

    def swap(u, blk, i, who):
        return pltpu.make_async_remote_copy(
            src_ref=slot(u, blk, spans[i], who),
            dst_ref=slot(u, blk, spans[i], who),
            send_sem=ysend.at[u, blk, i],
            recv_sem=yrecv.at[u, blk, i],
            device_id=peer,
            device_id_type=MESH,
        )

    def send_own(units_now, way):
        for u in units_now:
            for p in range(3):
                pl.when(passes(p, jnp.int32(way)))(lambda: along(u, z, p, way, True).start())

    D_UNITS = tuple(range(2, 2 + CHUNKS))
    send_own((0, 1), 0)
    send_own((0, 1), 1)
    pl.when(z == n - 1)(lambda: send_own(D_UNITS, 0))
    pl.when(z == 0)(lambda: send_own(D_UNITS, 1))

    locals_ = [
        pltpu.make_async_copy(wg_ref, bg.at[z], loc_sem.at[0]),
        pltpu.make_async_copy(wu_ref, bu.at[z], loc_sem.at[1]),
    ] + [
        pltpu.make_async_copy(wd_ref.at[:, pl.ds(j * cols, cols)], bd.at[z, j], loc_sem.at[2 + j])
        for j in range(CHUNKS)
    ]
    for copy in locals_:
        copy.start()

    step = 64

    def norm(src, base):
        @pl.loop(0, tokens // step)
        def _(i):
            at = pl.ds(pl.multiple_of(i * step, step), step)
            to = pl.ds(pl.multiple_of(base + i * step, step), step)
            wide = src[at, :].astype(F32)
            scale = lax.rsqrt(jnp.mean(wide * wide, axis=-1, keepdims=True) + 1e-06)
            normed[to, :] = (wide * scale * gain_ref[...]).astype(BF16)

    norm(tok_ref, 0)

    def add_dot(u, blk, first=False):
        total, held = (gate, bg) if u == 0 else (up, bu)

        def piece(start, size, base):
            @pl.loop(0, 4)
            def _(i):
                at = pl.ds(pl.multiple_of(i * half_t, half_t), half_t)
                left = normed[at, pl.ds(pl.multiple_of(blk * depth, depth), depth)]
                value = jnp.dot(left, held[blk, :, pl.ds(start, size)], preferred_element_type=F32)
                to = pl.ds(base, size)
                total[at, to] = value if first else total[at, to] + value

        piece(mine, most, 0)
        pl.when(has_mid)(lambda: piece(most, mid, most))

    def place(blk, j, who):
        return (
            pl.ds(pl.multiple_of(who * half_t, half_t), half_t),
            pl.ds(pl.multiple_of(blk * (cols * CHUNKS) + j * cols, cols), cols),
        )

    def to_mate(blk, j):
        return pltpu.make_async_remote_copy(
            part.at[blk, j, 1], r1.at[blk, j], psend.at[blk, j], precv.at[blk, j],
            device_id=mate, device_id_type=MESH)

    def to_across(blk, j):
        return pltpu.make_async_remote_copy(
            sx.at[blk, j], r2.at[blk, j], xsend.at[blk, j], xrecv.at[blk, j],
            device_id=across, device_id_type=MESH)

    def give(blk, j, who):
        return pltpu.make_async_remote_copy(
            outv.at[place(blk, j, who)], outv.at[place(blk, j, who)], qsend.at[blk, j], qrecv.at[blk, j],
            device_id=mate, device_id_type=MESH)

    def write(blk, j):
        at = pl.ds(pl.multiple_of(blk * (cols * CHUNKS) + j * cols, cols), cols)
        return pltpu.make_async_copy(outv.at[:, at], out_ref.at[:, at], osem.at[blk, j])

    def to_pair(blk, j):
        return pltpu.make_async_remote_copy(
            sbuf.at[blk, j, 1], rz.at[blk, j], wsend.at[blk, j], wrecv.at[blk, j],
            device_id=pair, device_id_type=MESH)

    def make_part(blk, j):
        def fill(with_mid):
            @pl.loop(0, 4)
            def _(i):
                side, which = i // 2, lax.rem(i, 2)
                whose = c + side - 2 * c * side
                at = pl.ds(pl.multiple_of(which * tokens + whose * half_t, half_t), half_t)
                value = jnp.dot(
                    hidden[at, pl.ds(0, most)], bd[blk, j, pl.ds(mine, most), :], preferred_element_type=F32)
                if with_mid:
                    value = value + jnp.dot(
                        hidden[at, pl.ds(most, mid)], bd[blk, j, pl.ds(most, mid), :], preferred_element_type=F32)
                part[blk, j, side, which] = value.astype(BF16)

        pl.when(has_mid)(lambda: fill(True))
        pl.when(jnp.logical_not(has_mid))(lambda: fill(False))
        to_mate(blk, j).start()

    def add_pair(blk, j):
        to_mate(blk, j).wait_recv()
        sbuf[blk, j] = (part[blk, j, 0].astype(F32) + r1[blk, j].astype(F32)).astype(BF16)
        to_pair(blk, j).start()

    def add_line(blk, j):
        to_pair(blk, j).wait_recv()
        sx[blk, j] = (sbuf[blk, j, 0].astype(F32) + rz[blk, j].astype(F32)).astype(BF16)
        to_across(blk, j).start()

    def finish(blk, j):
        to_across(blk, j).wait_recv()
        outv[place(blk, j, c)] = (sx[blk, j].astype(F32) + r2[blk, j].astype(F32)).astype(BF16)
        give(blk, j, c).start()

    def store(blk, j):
        give(blk, j, 1 - c).wait_recv()
        write(blk, j).start()

    def sides(k, body):
        @pl.loop(0, 2)
        def _(way):
            blk = z + k - 2 * k * way

            @pl.when(jnp.logical_and(blk >= 0, blk < n))
            def _():
                body(blk, way)

    def forward(u, k):
        def body(blk, way):
            for p in range(3):
                @pl.when(arrives(p, way))
                def _():
                    along(u, blk, p, way).wait_recv()
                    pl.when(passes(p, way))(lambda: along(u, blk, p, way).start())

            swap(u, blk, 0, y).start()
            pl.when(has_mid)(lambda: swap(u, blk, 1, y).start())

        sides(k, body)

    def use(u, k):
        def body(blk, way):
            swap(u, blk, 0, 1 - y).wait_recv()
            pl.when(has_mid)(lambda: swap(u, blk, 1, 1 - y).wait_recv())
            if u < 2:
                add_dot(u, blk)
            else:
                make_part(blk, u - 2)

        sides(k, body)
        if u >= 2:
            advance(k, u - 2)

    def reached(k, body):
        @pl.loop(0, 2)
        def _(way):
            blk = low + k + (1 - 2 * k) * way
            pl.when(jnp.logical_and(blk >= 0, blk < n))(lambda: body(blk))

    summed, crossing, closing = [], [], []

    def drain():
        if closing:
            k, j = closing.pop()
            reached(k, lambda blk: store(blk, j))
        if crossing:
            k, j = crossing.pop()
            reached(k, lambda blk: finish(blk, j))
            closing.append((k, j))
        if summed:
            k, j = summed.pop()
            reached(k, lambda blk: add_line(blk, j))
            crossing.append((k, j))

    def advance(k, j):
        drain()
        run(k, lambda blk: add_pair(blk, j))
        if k > 0:
            summed.append((k, j))

    def run(k, body):
        if k == 0:
            body(z)
        else:
            sides(k, lambda blk, way: body(blk))

    def middle():
        @pl.loop(0, 2 * tokens // step)
        def _(i):
            at = pl.ds(pl.multiple_of(i * step, step), step)
            value = gate[at, :]
            hidden[at, :] = (value / (1.0 + jnp.exp(-value)) * up[at, :]).astype(BF16)

        for j in range(CHUNKS):
            locals_[2 + j].wait()
            make_part(z, j)
            advance(0, j)

    token_move(t, pair, 0, True).wait_recv()
    for i, one in enumerate(others):
        token_move(t, one, 1 + i, False).start()

    def prepare():
        for d in (1, 2, 3):
            token_move(lax.rem(t + d, 4), mate, 0, False).wait_recv()
        norm(tokp, tokens)
        for u in (0, 1):
            locals_[u].wait()
            add_dot(u, z, first=True)

    events = [(u, k) for k in range(1, n) for u in (0, 1)]
    last_row = len(events)
    events += [(u, k) for k in range(1, n) for u in D_UNITS]
    for i in range(len(events) + LAG):
        if i < len(events):
            u, k = events[i]
            forward(u, k)
            if u == 1:
                pl.when(jnp.logical_and(n - 1 - z == k, z > 0))(lambda: send_own(D_UNITS, 0))
                pl.when(jnp.logical_and(z == k, z < n - 1))(lambda: send_own(D_UNITS, 1))
        if i == 0:
            prepare()
        if i >= LAG:
            use(*events[i - LAG])
            if i - LAG == last_row - 1:
                middle()
    for _ in range(3):
        drain()

    token_move(t, pair, 0, True).wait_send()
    for i, one in enumerate(others):
        token_move(t, one, 1 + i, False).wait_send()
    for u in range(2 + CHUNKS):
        for p in range(3):
            for way in (0, 1):
                pl.when(passes(p, jnp.int32(way)))(lambda: along(u, z, p, way, True).wait_send())
        for k in range(1, n):
            def sent(blk, way):
                for p in range(3):
                    pl.when(jnp.logical_and(arrives(p, way), passes(p, way)))(
                        lambda: along(u, blk, p, way).wait_send())
                swap(u, blk, 0, y).wait_send()
                pl.when(has_mid)(lambda: swap(u, blk, 1, y).wait_send())

            sides(k, sent)

    @pl.loop(0, n)
    def _(blk):
        for j in range(CHUNKS):
            to_mate(blk, j).wait_send()
            to_pair(blk, j).wait_send()
            to_across(blk, j).wait_send()
            give(blk, j, c).wait_send()
            write(blk, j).wait()


def fused(n, tokens, norm_gain, gate_weight, up_weight, down_weight):
    rows, width = tokens.shape
    depth, units = gate_weight.shape
    cols = down_weight.shape[1] // CHUNKS
    held = (units + 128) // 2
    dma = pltpu.SemaphoreType.DMA
    grid_of = (n, CHUNKS)
    hbm = pl.BlockSpec(memory_space=pl.ANY)
    vmem = pl.BlockSpec(memory_space=pltpu.VMEM)
    return pl.pallas_call(
        functools.partial(kernel, n),
        out_shape=jax.ShapeDtypeStruct((rows, width), BF16),
        in_specs=[vmem, vmem, hbm, hbm, hbm],
        out_specs=hbm,
        scratch_shapes=[
            pltpu.VMEM((rows, width), BF16),
            pltpu.VMEM((2 * rows, width), BF16),
            pltpu.VMEM((n, depth, units), BF16),
            pltpu.VMEM((n, depth, units), BF16),
            pltpu.VMEM((n, CHUNKS, units, cols), BF16),
            pltpu.VMEM((2 * rows, held), F32),
            pltpu.VMEM((2 * rows, held), F32),
            pltpu.VMEM((2 * rows, held), BF16),
            pltpu.VMEM((n, CHUNKS, 2, 2, rows // 2, cols), BF16),
            pltpu.VMEM((n, CHUNKS, 2, rows // 2, cols), BF16),
            pltpu.VMEM((n, CHUNKS, 2, rows // 2, cols), BF16),
            pltpu.VMEM((n, CHUNKS, rows // 2, cols), BF16),
            pltpu.VMEM((n, CHUNKS, rows // 2, cols), BF16),
            pltpu.VMEM((n, CHUNKS, rows // 2, cols), BF16),
            pltpu.VMEM((rows, width), BF16),
            dma((2 + CHUNKS,)),
            dma((2 + CHUNKS, n, 3, 2)),
            dma((2 + CHUNKS, n, 3)),
            dma((2 + CHUNKS, n, 2)),
            dma((2 + CHUNKS, n, 2)),
            dma((4,)),
            dma((4,)),
        ] + [dma(grid_of) for _ in range(9)],
        compiler_params=pltpu.CompilerParams(
            collective_id=0, has_side_effects=True, vmem_limit_bytes=60 * 2**20
        ),
    )(tokens, norm_gain.reshape(1, width), gate_weight, up_weight, down_weight)


def solution(mesh):
    n = mesh.shape["fs"]
    small = mesh.shape["rep"] == 2 and mesh.shape["tp"] == 4 and n == 4
    body = functools.partial(fused, n) if small else plain
    in_specs = (P(("rep", "fs"), None), P(), P("fs", "tp"), P("fs", "tp"), P("tp", "fs"))
    out_specs = P(("rep", "fs"), None)
    return jax.shard_map(
        body, mesh=mesh, in_specs=in_specs, out_specs=out_specs, check_vma=False
    )
```

time: 175 us -> 147 us (0.84)
  Pallas kernels: 172 us -> 143 us
    pallas_call x1, Pallas kernels: 172 us -> 143 us  [fused(): pl.pallas_call(functools.partial(kernel, n), out_shape=jax.ShapeDtypeStru...]
where the time goes in v2:
time: 147 us; the launch traced here: 146 us
  Pallas kernels  143 us (97%)
  local copies, waits for them, and re-layouts  3.16 us (2%)
    pallas_call x1, Pallas kernels, fused(): pl.pallas_call(functools.partial(kernel, n), out_shape=jax.ShapeDtypeStru...  143 us
    unnamed x1, local copies, waits for them, and re-layouts  3.16 us

profile of v2, /device:TPU:0, one launch (start us, length us, event | category | flops | bytes accessed | tf_op | source)
XLA Modules:
  0.0 146.0 jit_solution(17595181846958895348)
XLA Ops:
  0.0 142.8 %shard_map.55 = bf16[512,2048]{1,0:T(8,128)(2,1)} custom-call(bf16[512,2048]{1,0:T(8,128)(2,1)} %tok_ref.1, f32[1,2048]{1,0:T(1,128)} %bitcast.1, bf16[512,1408]{1,0:T(8,128)(2,1)} %wg_ref.1, bf16[512,1408]{1,0:T(8,128)(2,1)} %wu_ref.1, bf16[1408,512]{1,0:T(8,128)(2,1)} %wd_ref.1), custom_call_target="tpu_custom_call" | custom-call | tf_op jit(solution)/shard_map/pallas_call | solution.py:390
  142.9 3.2 %copy.7 = bf16[512,2048]{1,0:T(8,128)(2,1)} copy(bf16[512,2048]{1,0:T(8,128)(2,1)} %shard_map.55) | data formatting | bytes 4194304
